TPU v7x, 32 devices: a whole 2x2x4 slice. The times are simulated.
32 devices in a mesh: fs: 16 (over z, y, core), tp: 2 (over x).
Axes of the slice: x: 2, y: 2, z: 4, core: 2. Of those that a mesh axis runs over, the one named last changes fastest.
Arguments:
- saved_input: bfloat16 [8192, 3072], P('fs'), may hold values from -6 to 6
- output_cotangent: bfloat16 [8192, 3072], P('fs'), may hold values from -6 to 6
- recurrent_output: bfloat16 [8192, 1536], P('fs', 'tp'), may hold values from -6 to 6
- forget_logit: bfloat16 [8192, 1536], P('fs', 'tp'), may hold values from -12 to 12
- forget_cotangent: bfloat16 [8192, 1536], P('fs', 'tp'), may hold values from -6 to 6
- lower_bound: float32 [1536], P('tp'), may hold values from 0.2 to 0.9
- basis_in: bfloat16 [3072, 384], P('fs'), may hold values from -1.2629537 to 1.2629537
- basis_out: bfloat16 [3072, 384], P('fs'), may hold values from -1.2629537 to 1.2629537
- moment_in: float32 [384, 1536], P('fs', 'tp'), may hold values from -6 to 6
- second_in: float32 [384, 1536], P('fs', 'tp'), may hold values from 0.25 to 4
- moment_out: float32 [384, 1536], P('fs', 'tp'), may hold values from -6 to 6
- second_out: float32 [384, 1536], P('fs', 'tp'), may hold values from 0.25 to 4
- weight_in: float32 [3072, 1536], P('fs', 'tp'), may hold values from -0.109375 to 0.109375
- weight_out: float32 [1536, 3072], P('tp', 'fs'), may hold values from -0.15625 to 0.15625
Outputs:
- moment_in_new: float32 [384, 1536], P('fs', 'tp')
- second_in_new: float32 [384, 1536], P('fs', 'tp')
- moment_out_new: float32 [384, 1536], P('fs', 'tp')
- second_out_new: float32 [384, 1536], P('fs', 'tp')
- weight_in_new: float32 [3072, 1536], P('fs', 'tp')
- weight_out_new: float32 [1536, 3072], P('tp', 'fs')
- copy_in: bfloat16 [3072, 1536], P(None, 'tp')
- copy_out: bfloat16 [1536, 3072], P('tp')
All inputs are finite; a program needn't handle non-finite values.
Results may differ from a plain program's by a relative error of at most 0.0023.
Values may be sent and summed in bfloat16 or wider, within the bound.
A program may use at most 64 MiB of HBM per device.

v0:
```python
import jax
import jax.numpy as jnp
from jax import lax
from jax.sharding import PartitionSpec as P

HW = 1536
R = 384


def body(
    saved_input,
    output_cotangent,
    recurrent_output,
    forget_logit,
    forget_cotangent,
    lower_bound,
    basis_in,
    basis_out,
    moment_in,
    second_in,
    moment_out,
    second_out,
    weight_in,
    weight_out,
):
    sig = jax.nn.sigmoid(forget_logit.astype(jnp.float32))
    gate_cot = (
        forget_cotangent.astype(jnp.float32) * (1.0 - lower_bound)[None, :] * sig * (1.0 - sig)
    ).astype(jnp.bfloat16)
    full_in, full_out = (
        lax.all_gather(basis_in, "fs", axis=0, tiled=True),
        lax.all_gather(basis_out, "fs", axis=0, tiled=True),
    )
    coded_in = jnp.dot(saved_input, full_in, preferred_element_type=jnp.float32).astype(
        jnp.bfloat16
    )
    coded_out = jnp.dot(output_cotangent, full_out, preferred_element_type=jnp.float32).astype(
        jnp.bfloat16
    )
    units = recurrent_output.shape[1]
    contract = (((0,), (0,)), ((), ()))
    term_in = lax.dot_general(coded_in, gate_cot, contract, preferred_element_type=jnp.float32)
    term_out = lax.dot_general(
        coded_out, recurrent_output, contract, preferred_element_type=jnp.float32
    )
    lowrank = lax.psum_scatter(
        jnp.concatenate([term_in, term_out], axis=1), "fs", scatter_dimension=0, tiled=True
    )
    total = lax.psum(jnp.sum(lowrank * lowrank), ("fs", "tp"))
    clip = jnp.minimum(1.0, jnp.sqrt(jnp.float32(2 * R * HW)) * lax.rsqrt(total + 1e-06))
    grads = clip * lowrank
    moments = 0.8 * jnp.concatenate([moment_in, moment_out], axis=1) + 0.2 * grads
    seconds = 0.9 * jnp.concatenate([second_in, second_out], axis=1) + 0.1 * grads * grads
    stepping = moments / (jnp.sqrt(seconds) + 1e-08)
    whole_step = lax.all_gather(stepping, "fs", axis=0, tiled=True)
    update_in = jnp.dot(
        basis_in.astype(jnp.float32), whole_step[:, :units], precision=lax.Precision.HIGHEST
    )
    update_out = jnp.dot(
        whole_step[:, units:].T, basis_out.astype(jnp.float32).T, precision=lax.Precision.HIGHEST
    )
    weight_in_new = weight_in - 0.01 * update_in
    weight_out_new = weight_out - 0.01 * update_out
    copy_in, copy_out = (
        lax.all_gather(weight_in_new.astype(jnp.bfloat16), "fs", axis=0, tiled=True),
        lax.all_gather(weight_out_new.astype(jnp.bfloat16), "fs", axis=1, tiled=True),
    )
    return (
        moments[:, :units],
        seconds[:, :units],
        moments[:, units:],
        seconds[:, units:],
        weight_in_new,
        weight_out_new,
        copy_in,
        copy_out,
    )


def solution(mesh):
    return jax.shard_map(
        body,
        mesh=mesh,
        in_specs=(
            P("fs", None),
            P("fs", None),
            P("fs", "tp"),
            P("fs", "tp"),
            P("fs", "tp"),
            P("tp"),
            P("fs", None),
            P("fs", None),
            P("fs", "tp"),
            P("fs", "tp"),
            P("fs", "tp"),
            P("fs", "tp"),
            P("fs", "tp"),
            P("tp", "fs"),
        ),
        out_specs=(
            P("fs", "tp"),
            P("fs", "tp"),
            P("fs", "tp"),
            P("fs", "tp"),
            P("fs", "tp"),
            P("tp", "fs"),
            P(None, "tp"),
            P("tp", None),
        ),
        check_vma=False,
    )
```

profile of v0, /device:TPU:0, one launch (start us, length us, event | category | flops | bytes accessed | tf_op | source)
XLA Modules:
  0.0 377.6 jit_solution(13971637352224902390)
XLA Ops:
  7.2 0.0 copy-start
  7.2 0.0 all-gather.8.cloned.1.call-start
  7.2 0.7 all-gather.8.cloned.1.call-update
  7.9 0.0 all-gather.6.cloned.1.call-start
  8.0 0.7 all-gather.6.cloned.1.call-update
  8.7 0.0 reduce-scatter.2.cloned.1.call-start
  8.7 0.7 broadcast_subtract_fusion
  9.4 45.9 %all-gather.8.cloned.1.call-done = bf16[3072,384]{1,0:T(8,128)(2,1)} async-done(((bf16[192,384]{1,0:T(8,128)(2,1)}), bf16[3072,384]{1,0:T(8,128)(2,1)}) %all-gather.8.cloned.1.call-update) | async-done | bytes 2359312 | tf_op jit(solution)/shard_map/all_gather | solution.py:32
  55.3 0.0 copy-done
  55.3 5.2 %fusion.6 = f32[384,768]{1,0:T(8,128)} fusion(bf16[512,768]{1,0:T(8,128)(2,1)} %param.16, bf16[512,3072]{1,0:T(8,128)(2,1)S(1)} %copy-done, bf16[3072,384]{1,0:T(8,128)(2,1)} %all-gather.8.cloned.1.call-done), kind=kOutput, calls=%fused_computation.12 | convolution fusion | flops 1510146048 | bytes 7471104 | tf_op jit(solution)/shard_map/dot_general | solution.py:43
  60.5 38.1 %all-gather.6.cloned.1.call-done = bf16[3072,384]{1,0:T(8,128)(2,1)} async-done(((bf16[192,384]{1,0:T(8,128)(2,1)}), bf16[3072,384]{1,0:T(8,128)(2,1)}) %all-gather.6.cloned.1.call-update) | async-done | bytes 2359312 | tf_op jit(solution)/shard_map/all_gather | solution.py:31
  98.7 6.5 %fusion.5 = f32[384,768]{1,0:T(8,128)} fusion(bf16[512,3072]{1,0:T(8,128)(2,1)} %param.14, bf16[3072,384]{1,0:T(8,128)(2,1)} %all-gather.6.cloned.1.call-done, bf16[512,768]{1,0:T(8,128)(2,1)} %param.17, bf16[512,768]{1,0:T(8,128)(2,1)} %param.18, f32[768]{0:T(1024)S(1)} %broadcast_subtract_fusion), kind=kOutput, calls=%fused_computation.11 | convolution fusion | flops 1514078208 | bytes 8260608 | tf_op jit(solution)/shard_map/dot_general | solution.py:42
  105.2 3.3 pad_maximum_fusion
  108.4 0.0 copy-start.4
  108.5 0.0 copy-start.1
  108.5 0.0 reduce-scatter.2.cloned.1.call-update
  108.5 0.0 copy-start.2
  108.5 0.0 all-gather.10.cloned.1.call-start
  108.5 62.0 %reduce-scatter.2.cloned.1.call-done = f32[24,1536]{1,0:T(8,128)} async-done(((f32[384,1536]{1,0:T(8,128)}), f32[24,1536]{1,0:T(8,128)}) %reduce-scatter.2.cloned.1.call-update) | async-done | bytes 147472 | tf_op jit(solution)/shard_map/reduce_scatter | solution.py:46
  170.6 1.6 multiply_reduce_fusion
  172.1 40.0 %psum.7 = f32[]{:T(128)} all-reduce(f32[]{:T(128)} %multiply_reduce_fusion), channel_id=1, replica_groups=mesh['fs'=16,'tp'=2] {'fs','tp'}, use_global_device_ids=true, to_apply=%region_2.0 | all-reduce | flops 1 | bytes 8 | tf_op jit(solution)/shard_map/psum | solution.py:49
  212.8 0.0 copy-done.4
  212.8 1.8 add_divide_fusion
  214.6 0.0 all-gather.10.cloned.1.call-update
  214.6 0.0 all-gather.14.cloned.1.call-start
  214.7 41.8 %all-gather.10.cloned.1.call-done = f32[384,1536]{1,0:T(8,128)} async-done(((f32[24,1536]{1,0:T(8,128)}), f32[384,1536]{1,0:T(8,128)}) %all-gather.10.cloned.1.call-update) | async-done | bytes 2359312 | tf_op jit(solution)/shard_map/all_gather | solution.py:55
  256.5 0.0 copy-done.1
  256.5 3.0 fusion.16
  259.5 0.0 copy-start.3
  259.5 0.0 all-gather.14.cloned.1.call-update
  259.5 0.0 all-gather.12.cloned.1.call-start
  259.6 0.0 copy-done.2
  259.6 3.0 fusion.15
  262.6 0.0 all-gather.12.cloned.1.call-update
  262.6 0.0 copy-done.3
  262.6 1.6 fusion.13
  264.3 47.2 %all-gather.14.cloned.1.call-done = bf16[768,3072]{0,1:T(8,128)(2,1)} async-done(((bf16[768,192]{0,1:T(8,128)(2,1)}), bf16[768,3072]{0,1:T(8,128)(2,1)}) %all-gather.14.cloned.1.call-update) | async-done | bytes 4718608 | tf_op jit(solution)/shard_map/all_gather | solution.py:66
  311.5 6.6 %copy.22 = bf16[768,3072]{1,0:T(8,128)(2,1)} copy(bf16[768,3072]{0,1:T(8,128)(2,1)} %all-gather.14.cloned.1.call-done) | data formatting | bytes 9437184
  318.1 47.8 %all-gather.12.cloned.1.call-done = bf16[3072,768]{1,0:T(8,128)(2,1)} async-done(((bf16[192,768]{1,0:T(8,128)(2,1)}), bf16[3072,768]{1,0:T(8,128)(2,1)}) %all-gather.12.cloned.1.call-update) | async-done | bytes 4718608 | tf_op jit(solution)/shard_map/all_gather | solution.py:65
  365.9 4.8 %copy.24 = bf16[3072,768]{1,0:T(8,128)(2,1)} copy(bf16[3072,768]{1,0:T(8,128)(2,1)} %all-gather.12.cloned.1.call-done) | data formatting | bytes 9437184
Async XLA Ops:
  7.2 48.2 %copy-start = (bf16[512,3072]{1,0:T(8,128)(2,1)S(1)}, bf16[512,3072]{1,0:T(8,128)(2,1)}, u32[]{:S(2)}) copy-start(bf16[512,3072]{1,0:T(8,128)(2,1)} %param.15) | copy-start | bytes 9437188
  7.2 48.2 %all-gather.8.cloned.1.call-start = ((), (), s32[]{:S(2)}) async-start(), calls=%async_computation.2 | async-start | bytes 2506752 | tf_op jit(solution)/shard_map/all_gather | solution.py:32
  7.9 90.8 %all-gather.6.cloned.1.call-start = ((), (), s32[]{:S(2)}) async-start(), calls=%async_computation.1 | async-start | bytes 2506752 | tf_op jit(solution)/shard_map/all_gather | solution.py:31
  8.7 161.9 %reduce-scatter.2.cloned.1.call-start = ((), (), s32[]{:S(2)}) async-start(), calls=%async_computation.3 | async-start | bytes 2506752 | tf_op jit(solution)/shard_map/reduce_scatter | solution.py:46
  108.4 104.3 %copy-start.4 = (f32[24,768]{1,0:T(8,128)S(1)}, f32[24,768]{1,0:T(8,128)}, u32[]{:S(2)}) copy-start(f32[24,768]{1,0:T(8,128)} %param.25) | copy-start | bytes 221188
  108.5 148.0 %copy-start.1 = (bf16[192,384]{1,0:T(8,128)(2,1)S(1)}, bf16[192,384]{1,0:T(8,128)(2,1)}, u32[]{:S(2)}) copy-start(bf16[192,384]{1,0:T(8,128)(2,1)} %param.21) | copy-start | bytes 442372
  108.5 151.1 %copy-start.2 = (bf16[192,384]{1,0:T(8,128)(2,1)S(1)}, bf16[192,384]{1,0:T(8,128)(2,1)}, u32[]{:S(2)}) copy-start(bf16[192,384]{1,0:T(8,128)(2,1)} %param.20) | copy-start | bytes 442372
  108.5 148.0 %all-gather.10.cloned.1.call-start = ((), (), s32[]{:S(2)}) async-start(), calls=%async_computation.4 | async-start | bytes 2506752 | tf_op jit(solution)/shard_map/all_gather | solution.py:55
  214.6 96.9 %all-gather.14.cloned.1.call-start = ((), (), s32[]{:S(2)}) async-start(), calls=%async_computation.6 | async-start | bytes 5013504 | tf_op jit(solution)/shard_map/all_gather | solution.py:66
  259.5 3.1 copy-start.3
  259.5 106.4 %all-gather.12.cloned.1.call-start = ((), (), s32[]{:S(2)}) async-start(), calls=%async_computation.5 | async-start | bytes 5013504 | tf_op jit(solution)/shard_map/all_gather | solution.py:65
Sparse Core Ops, SparseCore 0:
  10.3 45.0 all-gather.7
  57.6 41.0 all-gather.5
  108.6 61.9 reduce-scatter.1
  214.8 41.6 all-gather.9
  259.6 51.8 all-gather.13
  314.2 51.6 all-gather.11
where the time goes:
time: 378 us
  waiting for transfers between devices  284 us (75%)
  blocking collectives  40 us (11%)
  matrix products  17.7 us (5%)
  between operations  14.9 us (4%)
  local copies, waits for them, and re-layouts  13.1 us (3%)
  other arithmetic  7.34 us (2%)
    reduce_scatter x1, waiting for transfers between devices, body(): lax.psum_scatter(jnp.concatenate([term_in, term_out], axis=1), 'fs', scat...  62 us
    all_gather x1, waiting for transfers between devices, body(): lax.all_gather(weight_in_new.astype(jnp.bfloat16), 'fs', axis=0, tiled=True)  47.8 us
    all_gather x1, waiting for transfers between devices, body(): lax.all_gather(weight_out_new.astype(jnp.bfloat16), 'fs', axis=1, tiled=T...  47.2 us
    all_gather x1, waiting for transfers between devices, body(): lax.all_gather(basis_out, 'fs', axis=0, tiled=True)  45.9 us
    all_gather x1, waiting for transfers between devices, body(): whole_step = lax.all_gather(stepping, 'fs', axis=0, tiled=True)  41.8 us
    psum x1, blocking collectives, body(): total = lax.psum(jnp.sum(lowrank * lowrank), ('fs', 'tp'))  40 us
    all_gather x1, waiting for transfers between devices, body(): lax.all_gather(basis_in, 'fs', axis=0, tiled=True)  38.1 us
    unnamed x12, local copies, waits for them, and re-layouts  11.5 us
  transfers between devices with their start and end apart: 6, of which 6 were waited for; matrix products, arithmetic and copies ran while one was open for 5% of the time, Pallas kernels for 0%

commit v1 on v0

--- a/solution.py
+++ b/solution.py
@@ -5,6 +5,16 @@
 
 HW = 1536
 R = 384
+
+
+def gather_by_hops(array, axis, dim):
+    size = lax.axis_size(axis)
+    held, blocks = (array, [array])
+    for _ in range(size - 1):
+        held = lax.ppermute(held, axis, [(i, (i + 1) % size) for i in range(size)])
+        blocks.insert(0, held)
+    merged = jnp.concatenate(blocks, axis=dim)
+    return jnp.roll(merged, (lax.axis_index(axis) + 1) * array.shape[dim], axis=dim)
 
 
 def body(
@@ -52,7 +62,7 @@
     moments = 0.8 * jnp.concatenate([moment_in, moment_out], axis=1) + 0.2 * grads
     seconds = 0.9 * jnp.concatenate([second_in, second_out], axis=1) + 0.1 * grads * grads
     stepping = moments / (jnp.sqrt(seconds) + 1e-08)
-    whole_step = lax.all_gather(stepping, "fs", axis=0, tiled=True)
+    whole_step = gather_by_hops(stepping, "fs", 0)
     update_in = jnp.dot(
         basis_in.astype(jnp.float32), whole_step[:, :units], precision=lax.Precision.HIGHEST
     )

time: 378 us -> 470 us (1.24)
  waiting for transfers between devices: 284 us -> 351 us
  local copies, waits for them, and re-layouts: 13.1 us -> 39.2 us
    ppermute x0 -> x15, waiting for transfers between devices: none -> 109 us  [gather_by_hops(): held = lax.ppermute(held, axis, [(i, (i + 1) % size) for i in range(size)])]
    all_gather x1 -> x0, waiting for transfers between devices: 41.8 us -> none  [body(): whole_step = lax.all_gather(stepping, 'fs', axis=0, tiled=True)]
    unnamed x12 -> x99, local copies, waits for them, and re-layouts: 11.5 us -> 37.5 us
  transfers between devices with their start and end apart: 6 -> 20, of which waited for: 6 -> 20; matrix products, arithmetic and copies ran while one was open for 5% -> 4% of each run, Pallas kernels for 0% -> 0%
where the time goes in v1:
time: 470 us; the launch traced here: 469 us
  waiting for transfers between devices  351 us (75%)
  blocking collectives  40 us (9%)
  local copies, waits for them, and re-layouts  39.2 us (8%)
  matrix products  16.5 us (4%)
  between operations  14.9 us (3%)
  other arithmetic  7.34 us (2%)
    ppermute x15, waiting for transfers between devices, gather_by_hops(): held = lax.ppermute(held, axis, [(i, (i + 1) % size) for i in range(size)])  109 us
    reduce_scatter x1, waiting for transfers between devices, body(): lax.psum_scatter(jnp.concatenate([term_in, term_out], axis=1), 'fs', scat...  62 us
    all_gather x1, waiting for transfers between devices, body(): lax.all_gather(weight_in_new.astype(jnp.bfloat16), 'fs', axis=0, tiled=True)  47.8 us
    all_gather x1, waiting for transfers between devices, body(): lax.all_gather(weight_out_new.astype(jnp.bfloat16), 'fs', axis=1, tiled=T...  46.4 us
    all_gather x1, waiting for transfers between devices, body(): lax.all_gather(basis_out, 'fs', axis=0, tiled=True)  45.9 us
    psum x1, blocking collectives, body(): total = lax.psum(jnp.sum(lowrank * lowrank), ('fs', 'tp'))  40 us
    all_gather x1, waiting for transfers between devices, body(): lax.all_gather(basis_in, 'fs', axis=0, tiled=True)  38.1 us
    unnamed x99, local copies, waits for them, and re-layouts  37.5 us
  transfers between devices with their start and end apart: 20, of which 20 were waited for; matrix products, arithmetic and copies ran while one was open for 4% of the time, Pallas kernels for 0%

profile of v1, /device:TPU:0, one launch (start us, length us, event | category | flops | bytes accessed | tf_op | source)
XLA Modules:
  0.0 469.2 jit_solution(163097248993950104)
XLA Ops:
  9.4 45.9 %all-gather.7.cloned.1.call-done = bf16[3072,384]{1,0:T(8,128)(2,1)} async-done(((bf16[192,384]{1,0:T(8,128)(2,1)}), bf16[3072,384]{1,0:T(8,128)(2,1)}) %all-gather.7.cloned.1.call-update) | async-done | bytes 2359312 | tf_op jit(solution)/shard_map/all_gather | solution.py:42
  55.3 5.2 %fusion.6 = f32[384,768]{1,0:T(8,128)} fusion(bf16[512,768]{1,0:T(8,128)(2,1)} %param.16, bf16[512,3072]{1,0:T(8,128)(2,1)S(1)} %copy-done, bf16[3072,384]{1,0:T(8,128)(2,1)} %all-gather.7.cloned.1.call-done), kind=kOutput, calls=%fused_computation.12 | convolution fusion | flops 1510146048 | bytes 7471104 | tf_op jit(solution)/shard_map/dot_general | solution.py:53
  60.5 38.1 %all-gather.5.cloned.1.call-done = bf16[3072,384]{1,0:T(8,128)(2,1)} async-done(((bf16[192,384]{1,0:T(8,128)(2,1)}), bf16[3072,384]{1,0:T(8,128)(2,1)}) %all-gather.5.cloned.1.call-update) | async-done | bytes 2359312 | tf_op jit(solution)/shard_map/all_gather | solution.py:41
  98.7 6.5 %fusion.5 = f32[384,768]{1,0:T(8,128)} fusion(bf16[512,3072]{1,0:T(8,128)(2,1)} %param.14, bf16[3072,384]{1,0:T(8,128)(2,1)} %all-gather.5.cloned.1.call-done, bf16[512,768]{1,0:T(8,128)(2,1)} %param.17, bf16[512,768]{1,0:T(8,128)(2,1)} %param.18, f32[768]{0:T(1024)S(1)} %broadcast_subtract_fusion), kind=kOutput, calls=%fused_computation.11 | convolution fusion | flops 1514078208 | bytes 8260608 | tf_op jit(solution)/shard_map/dot_general | solution.py:52
  105.2 3.3 pad_maximum_fusion
  108.6 62.0 %reduce-scatter.2.cloned.1.call-done = f32[24,1536]{1,0:T(8,128)} async-done(((f32[384,1536]{1,0:T(8,128)}), f32[24,1536]{1,0:T(8,128)}) %reduce-scatter.2.cloned.1.call-update) | async-done | bytes 147472 | tf_op jit(solution)/shard_map/reduce_scatter | solution.py:56
  170.6 1.6 multiply_reduce_fusion
  172.1 40.0 %psum.7 = f32[]{:T(128)} all-reduce(f32[]{:T(128)} %multiply_reduce_fusion), channel_id=1, replica_groups=mesh['fs'=16,'tp'=2] {'fs','tp'}, use_global_device_ids=true, to_apply=%region_2.0 | all-reduce | flops 1 | bytes 8 | tf_op jit(solution)/shard_map/psum | solution.py:59
  212.8 1.8 add_divide_fusion
  214.6 7.3 %collective-permute-done = f32[24,1536]{1,0:T(8,128)S(1)} collective-permute-done((f32[24,1536]{1,0:T(8,128)S(1)}, f32[24,1536]{1,0:T(8,128)S(1)}, u32[]{:S(2)}, u32[]{:S(2)}) %collective-permute-start) | collective-permute-done | bytes 147488 | tf_op jit(solution)/shard_map/ppermute | solution.py:14
  222.6 7.3 %collective-permute-done.1 = f32[24,1536]{1,0:T(8,128)S(1)} collective-permute-done((f32[24,1536]{1,0:T(8,128)S(1)}, f32[24,1536]{1,0:T(8,128)S(1)}, u32[]{:S(2)}, u32[]{:S(2)}) %collective-permute-start.1) | collective-permute-done | bytes 147488 | tf_op jit(solution)/shard_map/ppermute | solution.py:14
  230.5 7.3 %collective-permute-done.2 = f32[24,1536]{1,0:T(8,128)S(1)} collective-permute-done((f32[24,1536]{1,0:T(8,128)S(1)}, f32[24,1536]{1,0:T(8,128)S(1)}, u32[]{:S(2)}, u32[]{:S(2)}) %collective-permute-start.2) | collective-permute-done | bytes 147488 | tf_op jit(solution)/shard_map/ppermute | solution.py:14
  238.4 7.3 %collective-permute-done.3 = f32[24,1536]{1,0:T(8,128)S(1)} collective-permute-done((f32[24,1536]{1,0:T(8,128)S(1)}, f32[24,1536]{1,0:T(8,128)S(1)}, u32[]{:S(2)}, u32[]{:S(2)}) %collective-permute-start.3) | collective-permute-done | bytes 147488 | tf_op jit(solution)/shard_map/ppermute | solution.py:14
  246.3 7.3 %collective-permute-done.4 = f32[24,1536]{1,0:T(8,128)S(1)} collective-permute-done((f32[24,1536]{1,0:T(8,128)S(1)}, f32[24,1536]{1,0:T(8,128)S(1)}, u32[]{:S(2)}, u32[]{:S(2)}) %collective-permute-start.4) | collective-permute-done | bytes 147488 | tf_op jit(solution)/shard_map/ppermute | solution.py:14
  253.6 7.3 %collective-permute-done.5 = f32[24,1536]{1,0:T(8,128)S(1)} collective-permute-done((f32[24,1536]{1,0:T(8,128)S(1)}, f32[24,1536]{1,0:T(8,128)S(1)}, u32[]{:S(2)}, u32[]{:S(2)}) %collective-permute-start.5) | collective-permute-done | bytes 147488 | tf_op jit(solution)/shard_map/ppermute | solution.py:14
  261.5 7.3 %collective-permute-done.6 = f32[24,1536]{1,0:T(8,128)S(1)} collective-permute-done((f32[24,1536]{1,0:T(8,128)S(1)}, f32[24,1536]{1,0:T(8,128)S(1)}, u32[]{:S(2)}, u32[]{:S(2)}) %collective-permute-start.6) | collective-permute-done | bytes 147488 | tf_op jit(solution)/shard_map/ppermute | solution.py:14
  269.4 7.3 %collective-permute-done.7 = f32[24,1536]{1,0:T(8,128)S(1)} collective-permute-done((f32[24,1536]{1,0:T(8,128)S(1)}, f32[24,1536]{1,0:T(8,128)S(1)}, u32[]{:S(2)}, u32[]{:S(2)}) %collective-permute-start.7) | collective-permute-done | bytes 147488 | tf_op jit(solution)/shard_map/ppermute | solution.py:14
  277.4 7.3 %collective-permute-done.8 = f32[24,1536]{1,0:T(8,128)S(1)} collective-permute-done((f32[24,1536]{1,0:T(8,128)S(1)}, f32[24,1536]{1,0:T(8,128)S(1)}, u32[]{:S(2)}, u32[]{:S(2)}) %collective-permute-start.8) | collective-permute-done | bytes 147488 | tf_op jit(solution)/shard_map/ppermute | solution.py:14
  285.3 7.3 %collective-permute-done.9 = f32[24,1536]{1,0:T(8,128)S(1)} collective-permute-done((f32[24,1536]{1,0:T(8,128)S(1)}, f32[24,1536]{1,0:T(8,128)S(1)}, u32[]{:S(2)}, u32[]{:S(2)}) %collective-permute-start.9) | collective-permute-done | bytes 147488 | tf_op jit(solution)/shard_map/ppermute | solution.py:14
  293.2 7.3 %collective-permute-done.10 = f32[24,1536]{1,0:T(8,128)S(1)} collective-permute-done((f32[24,1536]{1,0:T(8,128)S(1)}, f32[24,1536]{1,0:T(8,128)S(1)}, u32[]{:S(2)}, u32[]{:S(2)}) %collective-permute-start.10) | collective-permute-done | bytes 147488 | tf_op jit(solution)/shard_map/ppermute | solution.py:14
  301.2 7.3 %collective-permute-done.11 = f32[24,1536]{1,0:T(8,128)S(1)} collective-permute-done((f32[24,1536]{1,0:T(8,128)S(1)}, f32[24,1536]{1,0:T(8,128)S(1)}, u32[]{:S(2)}, u32[]{:S(2)}) %collective-permute-start.11) | collective-permute-done | bytes 147488 | tf_op jit(solution)/shard_map/ppermute | solution.py:14
  309.1 7.3 %collective-permute-done.12 = f32[24,1536]{1,0:T(8,128)S(1)} collective-permute-done((f32[24,1536]{1,0:T(8,128)S(1)}, f32[24,1536]{1,0:T(8,128)S(1)}, u32[]{:S(2)}, u32[]{:S(2)}) %collective-permute-start.12) | collective-permute-done | bytes 147488 | tf_op jit(solution)/shard_map/ppermute | solution.py:14
  317.0 7.4 %collective-permute-done.13 = f32[24,1536]{1,0:T(8,128)} collective-permute-done((f32[24,1536]{1,0:T(8,128)S(1)}, f32[24,1536]{1,0:T(8,128)}, u32[]{:S(2)}, u32[]{:S(2)}) %collective-permute-start.13) | collective-permute-done | bytes 147488 | tf_op jit(solution)/shard_map/ppermute | solution.py:14
  324.5 7.5 %collective-permute-done.14 = f32[24,1536]{1,0:T(8,128)} collective-permute-done((f32[24,1536]{1,0:T(8,128)}, f32[24,1536]{1,0:T(8,128)}, u32[]{:S(2)}, u32[]{:S(2)}) %collective-permute-start.14) | collective-permute-done | bytes 147488 | tf_op jit(solution)/shard_map/ppermute | solution.py:14
  332.9 0.9 constant_dynamic-update-slice_fusion.30
  333.8 0.9 constant_dynamic-update-slice_fusion.29
  334.7 0.9 constant_dynamic-update-slice_fusion.28
  335.7 0.9 constant_dynamic-update-slice_fusion.27
  336.6 0.9 constant_dynamic-update-slice_fusion.26
  337.5 0.9 constant_dynamic-update-slice_fusion.25
  338.4 0.9 constant_dynamic-update-slice_fusion.24
  339.4 0.9 constant_dynamic-update-slice_fusion.23
  340.3 0.9 constant_dynamic-update-slice_fusion.22
  341.3 1.0 constant_dynamic-update-slice_fusion.20
  342.2 0.9 constant_dynamic-update-slice_fusion.19
  343.1 0.9 constant_dynamic-update-slice_fusion.18
  344.1 0.9 constant_dynamic-update-slice_fusion.17
  345.0 0.9 constant_dynamic-update-slice_fusion.15
  345.9 0.9 constant_dynamic-update-slice_fusion.14
  347.1 0.9 constant_dynamic-update-slice_fusion.5
  348.2 2.2 copy-done.1
  350.4 1.8 fusion.17
  352.2 3.1 fusion.16
  355.3 1.7 fusion.14
  357.0 46.4 %all-gather.11.cloned.1.call-done = bf16[768,3072]{0,1:T(8,128)(2,1)} async-done(((bf16[768,192]{0,1:T(8,128)(2,1)}), bf16[768,3072]{0,1:T(8,128)(2,1)}) %all-gather.11.cloned.1.call-update) | async-done | bytes 4718608 | tf_op jit(solution)/shard_map/all_gather | solution.py:76
  403.5 6.6 %copy.22 = bf16[768,3072]{1,0:T(8,128)(2,1)} copy(bf16[768,3072]{0,1:T(8,128)(2,1)} %all-gather.11.cloned.1.call-done) | data formatting | bytes 9437184
  410.1 47.8 %all-gather.9.cloned.1.call-done = bf16[3072,768]{1,0:T(8,128)(2,1)} async-done(((bf16[192,768]{1,0:T(8,128)(2,1)}), bf16[3072,768]{1,0:T(8,128)(2,1)}) %all-gather.9.cloned.1.call-update) | async-done | bytes 4718608 | tf_op jit(solution)/shard_map/all_gather | solution.py:75
  457.9 4.8 %copy.55 = bf16[3072,768]{1,0:T(8,128)(2,1)} copy(bf16[3072,768]{1,0:T(8,128)(2,1)} %all-gather.9.cloned.1.call-done) | data formatting | bytes 9437184
  (107 shorter events, 11.5 us)
Async XLA Ops:
  7.2 48.2 %copy-start = (bf16[512,3072]{1,0:T(8,128)(2,1)S(1)}, bf16[512,3072]{1,0:T(8,128)(2,1)}, u32[]{:S(2)}) copy-start(bf16[512,3072]{1,0:T(8,128)(2,1)} %param.15) | copy-start | bytes 9437188
  7.2 48.2 %all-gather.7.cloned.1.call-start = ((), (), s32[]{:S(2)}) async-start(), calls=%async_computation.2 | async-start | bytes 2506752 | tf_op jit(solution)/shard_map/all_gather | solution.py:42
  7.9 90.8 %all-gather.5.cloned.1.call-start = ((), (), s32[]{:S(2)}) async-start(), calls=%async_computation.1 | async-start | bytes 2506752 | tf_op jit(solution)/shard_map/all_gather | solution.py:41
  8.7 161.9 %reduce-scatter.2.cloned.1.call-start = ((), (), s32[]{:S(2)}) async-start(), calls=%async_computation.3 | async-start | bytes 2506752 | tf_op jit(solution)/shard_map/reduce_scatter | solution.py:56
  105.2 107.7 %copy-start.30 = (f32[24,768]{1,0:T(8,128)S(1)}, f32[24,768]{1,0:T(8,128)}, u32[]{:S(2)}) copy-start(f32[24,768]{1,0:T(8,128)} %param.25) | copy-start | bytes 221188
  105.2 107.7 %copy-start.31 = (f32[24,768]{1,0:T(8,128)S(1)}, f32[24,768]{1,0:T(8,128)}, u32[]{:S(2)}) copy-start(f32[24,768]{1,0:T(8,128)} %param.23) | copy-start | bytes 221188
  105.2 107.7 %copy-start.32 = (f32[24,768]{1,0:T(8,128)S(1)}, f32[24,768]{1,0:T(8,128)}, u32[]{:S(2)}) copy-start(f32[24,768]{1,0:T(8,128)} %param.24) | copy-start | bytes 221188
  108.5 295.0 %all-gather.11.cloned.1.call-start = ((), (), s32[]{:S(2)}) async-start(), calls=%async_computation.5 | async-start | bytes 5013504 | tf_op jit(solution)/shard_map/all_gather | solution.py:76
  214.6 7.3 %collective-permute-start = (f32[24,1536]{1,0:T(8,128)S(1)}, f32[24,1536]{1,0:T(8,128)S(1)}, u32[]{:S(2)}, u32[]{:S(2)}) collective-permute-start(f32[24,1536]{1,0:T(8,128)S(1)} %get-tuple-element.16), channel_id=1, source_target_pairs={{0,2},{2,4},{4,6},{6,8},{8,10},{10,12},{12,14},{14,16},{16,18},{18... | collective-permute-start | bytes 442376 | tf_op jit(solution)/shard_map/ppermute | solution.py:14
  221.9 0.7 copy-start.5
  222.6 7.3 %collective-permute-start.1 = (f32[24,1536]{1,0:T(8,128)S(1)}, f32[24,1536]{1,0:T(8,128)S(1)}, u32[]{:S(2)}, u32[]{:S(2)}) collective-permute-start(f32[24,1536]{1,0:T(8,128)S(1)} %collective-permute-done), channel_id=1, source_target_pairs={{0,2},{2,4},{4,6},{6,8},{8,10},{10,12},{12,14},{14,16},{16,18},{18... | collective-permute-start | bytes 442376 | tf_op jit(solution)/shard_map/ppermute | solution.py:14
  229.8 0.7 copy-start.7
  230.5 7.3 %collective-permute-start.2 = (f32[24,1536]{1,0:T(8,128)S(1)}, f32[24,1536]{1,0:T(8,128)S(1)}, u32[]{:S(2)}, u32[]{:S(2)}) collective-permute-start(f32[24,1536]{1,0:T(8,128)S(1)} %collective-permute-done.1), channel_id=1, source_target_pairs={{0,2},{2,4},{4,6},{6,8},{8,10},{10,12},{12,14},{14,16},{16,18},{18... | collective-permute-start | bytes 442376 | tf_op jit(solution)/shard_map/ppermute | solution.py:14
  238.4 7.3 %collective-permute-start.3 = (f32[24,1536]{1,0:T(8,128)S(1)}, f32[24,1536]{1,0:T(8,128)S(1)}, u32[]{:S(2)}, u32[]{:S(2)}) collective-permute-start(f32[24,1536]{1,0:T(8,128)S(1)} %collective-permute-done.2), channel_id=1, source_target_pairs={{0,2},{2,4},{4,6},{6,8},{8,10},{10,12},{12,14},{14,16},{16,18},{18... | collective-permute-start | bytes 442376 | tf_op jit(solution)/shard_map/ppermute | solution.py:14
  245.7 0.7 copy-start.11
  246.3 7.3 %collective-permute-start.4 = (f32[24,1536]{1,0:T(8,128)S(1)}, f32[24,1536]{1,0:T(8,128)S(1)}, u32[]{:S(2)}, u32[]{:S(2)}) collective-permute-start(f32[24,1536]{1,0:T(8,128)S(1)} %collective-permute-done.3), channel_id=1, source_target_pairs={{0,2},{2,4},{4,6},{6,8},{8,10},{10,12},{12,14},{14,16},{16,18},{18... | collective-permute-start | bytes 442376 | tf_op jit(solution)/shard_map/ppermute | solution.py:14
  253.6 87.6 %copy-start.13 = (f32[24,1536]{1,0:T(8,128)}, f32[24,1536]{1,0:T(8,128)S(1)}, u32[]{:S(2)}) copy-start(f32[24,1536]{1,0:T(8,128)S(1)} %collective-permute-done.4) | copy-start | bytes 442372
  253.6 7.3 %collective-permute-start.5 = (f32[24,1536]{1,0:T(8,128)S(1)}, f32[24,1536]{1,0:T(8,128)S(1)}, u32[]{:S(2)}, u32[]{:S(2)}) collective-permute-start(f32[24,1536]{1,0:T(8,128)S(1)} %collective-permute-done.4), channel_id=1, source_target_pairs={{0,2},{2,4},{4,6},{6,8},{8,10},{10,12},{12,14},{14,16},{16,18},{18... | collective-permute-start | bytes 442376 | tf_op jit(solution)/shard_map/ppermute | solution.py:14
  260.9 0.7 copy-start.14
  261.5 7.3 %collective-permute-start.6 = (f32[24,1536]{1,0:T(8,128)S(1)}, f32[24,1536]{1,0:T(8,128)S(1)}, u32[]{:S(2)}, u32[]{:S(2)}) collective-permute-start(f32[24,1536]{1,0:T(8,128)S(1)} %collective-permute-done.5), channel_id=1, source_target_pairs={{0,2},{2,4},{4,6},{6,8},{8,10},{10,12},{12,14},{14,16},{16,18},{18... | collective-permute-start | bytes 442376 | tf_op jit(solution)/shard_map/ppermute | solution.py:14
  269.4 7.3 %collective-permute-start.7 = (f32[24,1536]{1,0:T(8,128)S(1)}, f32[24,1536]{1,0:T(8,128)S(1)}, u32[]{:S(2)}, u32[]{:S(2)}) collective-permute-start(f32[24,1536]{1,0:T(8,128)S(1)} %collective-permute-done.6), channel_id=1, source_target_pairs={{0,2},{2,4},{4,6},{6,8},{8,10},{10,12},{12,14},{14,16},{16,18},{18... | collective-permute-start | bytes 442376 | tf_op jit(solution)/shard_map/ppermute | solution.py:14
  277.4 7.3 %collective-permute-start.8 = (f32[24,1536]{1,0:T(8,128)S(1)}, f32[24,1536]{1,0:T(8,128)S(1)}, u32[]{:S(2)}, u32[]{:S(2)}) collective-permute-start(f32[24,1536]{1,0:T(8,128)S(1)} %collective-permute-done.7), channel_id=1, source_target_pairs={{0,2},{2,4},{4,6},{6,8},{8,10},{10,12},{12,14},{14,16},{16,18},{18... | collective-permute-start | bytes 442376 | tf_op jit(solution)/shard_map/ppermute | solution.py:14
  284.6 0.7 copy-start.20
  285.3 7.3 %collective-permute-start.9 = (f32[24,1536]{1,0:T(8,128)S(1)}, f32[24,1536]{1,0:T(8,128)S(1)}, u32[]{:S(2)}, u32[]{:S(2)}) collective-permute-start(f32[24,1536]{1,0:T(8,128)S(1)} %collective-permute-done.8), channel_id=1, source_target_pairs={{0,2},{2,4},{4,6},{6,8},{8,10},{10,12},{12,14},{14,16},{16,18},{18... | collective-permute-start | bytes 442376 | tf_op jit(solution)/shard_map/ppermute | solution.py:14
  293.2 7.3 %collective-permute-start.10 = (f32[24,1536]{1,0:T(8,128)S(1)}, f32[24,1536]{1,0:T(8,128)S(1)}, u32[]{:S(2)}, u32[]{:S(2)}) collective-permute-start(f32[24,1536]{1,0:T(8,128)S(1)} %collective-permute-done.9), channel_id=1, source_target_pairs={{0,2},{2,4},{4,6},{6,8},{8,10},{10,12},{12,14},{14,16},{16,18},{18... | collective-permute-start | bytes 442376 | tf_op jit(solution)/shard_map/ppermute | solution.py:14
  300.5 0.7 copy-start.24
  301.1 7.3 %collective-permute-start.11 = (f32[24,1536]{1,0:T(8,128)S(1)}, f32[24,1536]{1,0:T(8,128)S(1)}, u32[]{:S(2)}, u32[]{:S(2)}) collective-permute-start(f32[24,1536]{1,0:T(8,128)S(1)} %collective-permute-done.10), channel_id=1, source_target_pairs={{0,2},{2,4},{4,6},{6,8},{8,10},{10,12},{12,14},{14,16},{16,18},{18... | collective-permute-start | bytes 442376 | tf_op jit(solution)/shard_map/ppermute | solution.py:14
  309.1 7.3 %collective-permute-start.12 = (f32[24,1536]{1,0:T(8,128)S(1)}, f32[24,1536]{1,0:T(8,128)S(1)}, u32[]{:S(2)}, u32[]{:S(2)}) collective-permute-start(f32[24,1536]{1,0:T(8,128)S(1)} %collective-permute-done.11), channel_id=1, source_target_pairs={{0,2},{2,4},{4,6},{6,8},{8,10},{10,12},{12,14},{14,16},{16,18},{18... | collective-permute-start | bytes 442376 | tf_op jit(solution)/shard_map/ppermute | solution.py:14
  316.3 0.7 copy-start.28
  317.0 7.4 %collective-permute-start.13 = (f32[24,1536]{1,0:T(8,128)S(1)}, f32[24,1536]{1,0:T(8,128)}, u32[]{:S(2)}, u32[]{:S(2)}) collective-permute-start(f32[24,1536]{1,0:T(8,128)S(1)} %collective-permute-done.12), channel_id=1, source_target_pairs={{0,2},{2,4},{4,6},{6,8},{8,10},{10,12},{12,14},{14,16},{16,18},{18... | collective-permute-start | bytes 442376 | tf_op jit(solution)/shard_map/ppermute | solution.py:14
  324.4 7.6 %collective-permute-start.14 = (f32[24,1536]{1,0:T(8,128)}, f32[24,1536]{1,0:T(8,128)}, u32[]{:S(2)}, u32[]{:S(2)}) collective-permute-start(f32[24,1536]{1,0:T(8,128)} %collective-permute-done.13), channel_id=1, source_target_pairs={{0,2},{2,4},{4,6},{6,8},{8,10},{10,12},{12,14},{14,16},{16,18},{18... | collective-permute-start | bytes 442376 | tf_op jit(solution)/shard_map/ppermute | solution.py:14
  324.4 22.5 %copy-start.29 = (f32[24,1536]{1,0:T(8,128)S(1)}, f32[24,1536]{1,0:T(8,128)}, u32[]{:S(2)}) copy-start(f32[24,1536]{1,0:T(8,128)} %copy-done.28) | copy-start | bytes 442372
  324.4 22.5 %copy-start.27 = (f32[24,1536]{1,0:T(8,128)S(1)}, f32[24,1536]{1,0:T(8,128)}, u32[]{:S(2)}) copy-start(f32[24,1536]{1,0:T(8,128)} %copy-done.26) | copy-start | bytes 442372
  324.4 22.5 %copy-start.25 = (f32[24,1536]{1,0:T(8,128)S(1)}, f32[24,1536]{1,0:T(8,128)}, u32[]{:S(2)}) copy-start(f32[24,1536]{1,0:T(8,128)} %copy-done.24) | copy-start | bytes 442372
  324.4 22.6 %copy-start.23 = (f32[24,1536]{1,0:T(8,128)S(1)}, f32[24,1536]{1,0:T(8,128)}, u32[]{:S(2)}) copy-start(f32[24,1536]{1,0:T(8,128)} %copy-done.22) | copy-start | bytes 442372
  324.4 22.6 %copy-start.21 = (f32[24,1536]{1,0:T(8,128)S(1)}, f32[24,1536]{1,0:T(8,128)}, u32[]{:S(2)}) copy-start(f32[24,1536]{1,0:T(8,128)} %copy-done.20) | copy-start | bytes 442372
  324.4 22.6 %copy-start.19 = (f32[24,1536]{1,0:T(8,128)S(1)}, f32[24,1536]{1,0:T(8,128)}, u32[]{:S(2)}) copy-start(f32[24,1536]{1,0:T(8,128)} %copy-done.18) | copy-start | bytes 442372
  324.4 22.6 %copy-start.17 = (f32[24,1536]{1,0:T(8,128)S(1)}, f32[24,1536]{1,0:T(8,128)}, u32[]{:S(2)}) copy-start(f32[24,1536]{1,0:T(8,128)} %copy-done.16) | copy-start | bytes 442372
  324.4 22.6 %copy-start.15 = (f32[24,1536]{1,0:T(8,128)S(1)}, f32[24,1536]{1,0:T(8,128)}, u32[]{:S(2)}) copy-start(f32[24,1536]{1,0:T(8,128)} %copy-done.14) | copy-start | bytes 442372
  324.4 23.6 %copy-start.12 = (f32[24,1536]{1,0:T(8,128)S(1)}, f32[24,1536]{1,0:T(8,128)}, u32[]{:S(2)}) copy-start(f32[24,1536]{1,0:T(8,128)} %copy-done.11) | copy-start | bytes 442372
  324.5 23.6 %copy-start.10 = (f32[24,1536]{1,0:T(8,128)S(1)}, f32[24,1536]{1,0:T(8,128)}, u32[]{:S(2)}) copy-start(f32[24,1536]{1,0:T(8,128)} %copy-done.9) | copy-start | bytes 442372
  324.5 23.6 %copy-start.8 = (f32[24,1536]{1,0:T(8,128)S(1)}, f32[24,1536]{1,0:T(8,128)}, u32[]{:S(2)}) copy-start(f32[24,1536]{1,0:T(8,128)} %copy-done.7) | copy-start | bytes 442372
  324.5 23.7 %copy-start.6 = (f32[24,1536]{1,0:T(8,128)S(1)}, f32[24,1536]{1,0:T(8,128)}, u32[]{:S(2)}) copy-start(f32[24,1536]{1,0:T(8,128)} %copy-done.5) | copy-start | bytes 442372
  324.5 25.9 %copy-start.2 = (bf16[192,384]{1,0:T(8,128)(2,1)S(1)}, bf16[192,384]{1,0:T(8,128)(2,1)}, u32[]{:S(2)}) copy-start(bf16[192,384]{1,0:T(8,128)(2,1)} %param.21) | copy-start | bytes 442372
  324.5 25.9 %copy-start.4 = (f32[768,192]{0,1:T(8,128)S(1)}, f32[768,192]{0,1:T(8,128)}, u32[]{:S(2)}) copy-start(f32[768,192]{0,1:T(8,128)} %param.27) | copy-start | bytes 1769476
  341.2 11.0 %copy-start.3 = (bf16[192,384]{1,0:T(8,128)(2,1)S(1)}, bf16[192,384]{1,0:T(8,128)(2,1)}, u32[]{:S(2)}) copy-start(bf16[192,384]{1,0:T(8,128)(2,1)} %param.20) | copy-start | bytes 442372
  348.2 2.2 copy-start.1
  352.2 105.7 %all-gather.9.cloned.1.call-start = ((), (), s32[]{:S(2)}) async-start(), calls=%async_computation.4 | async-start | bytes 5013504 | tf_op jit(solution)/shard_map/all_gather | solution.py:75
  (5 other events, 3.3 us)
Sparse Core Ops, SparseCore 0:
  10.3 45.0 all-gather.6
  57.6 41.0 all-gather.4
  108.6 61.9 reduce-scatter.1
  352.3 51.1 all-gather.10
  406.2 51.6 all-gather.8
